TPU v7x, 256 devices: a 4x2x16 block of a 4x16x16 slice. The times are simulated.
256 devices in a mesh: grp: 2 (over y), fs: 16 (over z), tp: 8 (over x, core).
Axes of the slice: x: 4, y: 2, z: 16, core: 2. Of those that a mesh axis runs over, the one named last changes fastest.
The devices are a block of a 4x16x16 slice.
Arguments:
- layer_input: bfloat16 [12288, 2048], P(('grp', 'fs'), 'tp'), parts along dimension 0, may hold values from -6 to 6
- first_gain: bfloat16 [1, 2048], P(None, 'tp'), may hold values from 0.099609375 to 1.8984375
- ffn_gate_w: bfloat16 [2048, 6144], P('fs', 'tp'), may hold values from -0.125 to 0.125
- ffn_up_w: bfloat16 [2048, 6144], P('fs', 'tp'), may hold values from -0.125 to 0.125
- ffn_down_w: bfloat16 [6144, 2048], P('tp', 'fs'), may hold values from -0.078125 to 0.078125
- mixer_gain: bfloat16 [1, 2048], P(None, 'tp'), may hold values from 0.099609375 to 1.8984375
- pool_in_w: bfloat16 [2048, 1024], P('fs', 'tp'), may hold values from -0.125 to 0.125
- mixer_gate_w: bfloat16 [2048, 2048], P('fs', 'tp'), may hold values from -0.125 to 0.125
- group_mix_w: bfloat16 [8, 128, 128], P('tp'), may hold values from -0.5 to 0.5
- pool_scale: float32 [1, 1024], P(None, 'tp'), may hold values from 0.1 to 1.9
- mixer_out_w: bfloat16 [1024, 2048], P('tp', 'fs'), may hold values from -0.1875 to 0.1875
- second_gain: bfloat16 [1, 2048], P(None, 'tp'), may hold values from 0.099609375 to 1.8984375
Outputs:
- layer_output: bfloat16 [12288, 2048], P(('grp', 'fs'), 'tp'), parts along dimension 0
There are 2 independent parts, one for each index of `grp`. A program takes and returns all parts, laid end to end along the dimension named above; an argument that names none is the same for every part. Nothing has to cross between parts.
All inputs are finite; a program needn't handle non-finite values.
Results may differ from a plain program's by a relative error of at most 0.015.
Values may be sent and summed in bfloat16 or wider, within the bound.
A program may use at most 64 MiB of HBM per device.

v0:
```python
import jax
import jax.numpy as jnp
from jax import lax
from jax.sharding import Mesh
from jax.sharding import PartitionSpec as P

TP = ("tp_0", "tp_1")


def from_everyone(value, axis):
    length = lax.axis_size(axis)
    return lax.all_to_all(
        jnp.broadcast_to(value[None], (length, *value.shape)), axis, 0, 0, tiled=True
    )


def joined_along(tiles, dim):
    shape = list(tiles.shape[1:])
    shape[dim] *= tiles.shape[0]
    return jnp.moveaxis(tiles, 0, dim).reshape(shape)


def whole_of(value, axes, dim):
    far, near = axes
    initial = from_everyone(value, far)
    tiles = jnp.swapaxes(from_everyone(initial, near), 0, 1)
    return joined_along(tiles.reshape(-1, *value.shape), dim)


def in_one_piece(arrays, axis, dim, along):
    widths = [a.shape[along] for a in arrays]
    both = jnp.concatenate(arrays, axis=along)
    filled = whole_of(both, axis, dim)
    return tuple(jnp.split(filled, [sum(widths[:k]) for k in range(1, len(widths))], axis=along))


def in_blocks(value, dim, length):
    before, after = (value.shape[:dim], value.shape[dim + 1 :])
    return jnp.moveaxis(value.reshape(*before, length, -1, *after), dim, 0)


def summed_on_arrival(value, axis, dim):
    tiles = in_blocks(value, dim, lax.axis_size(axis))
    arrived = lax.all_to_all(tiles, axis, split_axis=0, concat_axis=0, tiled=True)
    return arrived.astype(jnp.float32).sum(axis=0)


def sent_together(arrays, axis, dim, along):
    ends, at = ([], 0)
    for a in arrays[:-1]:
        at += a.shape[along]
        ends.append(at)
    both = jnp.concatenate(arrays, axis=along)
    return tuple(jnp.split(lax.all_gather(both, axis, axis=dim, tiled=True), ends, axis=along))


def gather_directly(value, axis, dim):
    return joined_along(from_everyone(value, axis), dim)


def norm_rows(values, gain):
    gathered, gain_whole = in_one_piece((values, gain), ("tp_0", "tp_1"), 1, 0)
    widened = gathered.astype(jnp.float32)
    scaled = (widened * gain_whole.astype(jnp.float32)).astype(jnp.bfloat16)
    factor = lax.rsqrt(jnp.mean(widened * widened, axis=1, keepdims=True) + 1e-06)
    return (scaled, factor)


def column_sums(partial_value):
    return summed_on_arrival(partial_value.astype(jnp.bfloat16), TP, 1)


def add_pair(scaled, pieces):
    first_sum = jnp.dot(scaled, pieces[0], preferred_element_type=jnp.float32)
    second_sum = jnp.dot(scaled, pieces[1], preferred_element_type=jnp.float32)
    return (first_sum, second_sum)


def per_device(
    layer_input,
    first_gain,
    ffn_gate_w,
    ffn_up_w,
    ffn_down_w,
    mixer_gain,
    pool_in_w,
    mixer_gate_w,
    group_mix_w,
    pool_scale,
    mixer_out_w,
    second_gain,
):
    row_count = layer_input.shape[0]
    gate_whole, up_whole = sent_together((ffn_gate_w, ffn_up_w), "fs", 0, 1)
    down_whole = lax.all_gather(ffn_down_w, "fs", axis=1, tiled=True)

    def feed_forward(values, gain):
        scaled, factor = norm_rows(values, gain)
        gate_pre = factor * jnp.dot(scaled, gate_whole, preferred_element_type=jnp.float32)
        up_pre = factor * jnp.dot(scaled, up_whole, preferred_element_type=jnp.float32)
        hidden = (jax.nn.silu(gate_pre) * up_pre).astype(jnp.bfloat16)
        return jnp.dot(hidden, down_whole, preferred_element_type=jnp.float32)

    first = (
        layer_input.astype(jnp.float32) + 0.5 * column_sums(feed_forward(layer_input, first_gain))
    ).astype(jnp.bfloat16)
    scaled, factor = norm_rows(first, mixer_gain)
    pool_sum, gate_sum = add_pair(scaled, sent_together((pool_in_w, mixer_gate_w), "fs", 0, 1))
    pool_pre = (factor * pool_sum).astype(jnp.bfloat16)
    gate_logit = factor * gate_sum
    group_count = group_mix_w.shape[0]
    group_width = group_mix_w.shape[1]
    first_group = lax.axis_index(TP) * group_count
    values = pool_pre.astype(jnp.float32).reshape(row_count, group_count, group_width)
    running = jnp.cumsum(values, axis=0)
    positions = jnp.arange(row_count, dtype=jnp.int32)
    windows = 2 ** (1 + (first_group + jnp.arange(group_count, dtype=jnp.int32)) % 4)
    chosen = jnp.zeros_like(values)
    for span in (2, 4, 8, 16):
        lagged = jnp.pad(running, ((span, 0), (0, 0), (0, 0)))[:row_count]
        counts = jnp.minimum(positions + 1, span).astype(jnp.float32)[:, None, None]
        means = (running - lagged) / counts
        chosen = jnp.where((windows == span)[None, :, None], means, chosen)
    trail = (chosen - values).astype(jnp.bfloat16)
    mixed = jnp.einsum("tgc,gcd->tgd", trail, group_mix_w, preferred_element_type=jnp.float32)
    pooled = (mixed.reshape(row_count, group_count * group_width) * pool_scale).astype(jnp.bfloat16)
    lifted = column_sums(
        jnp.dot(pooled, gather_directly(mixer_out_w, "fs", 1), preferred_element_type=jnp.float32)
    )
    second = (first.astype(jnp.float32) + jax.nn.sigmoid(gate_logit) * lifted).astype(jnp.bfloat16)
    result = second.astype(jnp.float32) + 0.5 * column_sums(feed_forward(second, second_gain))
    return result.astype(jnp.bfloat16)


def solution(mesh):
    finer = Mesh(
        mesh.devices.reshape(mesh.shape["grp"], mesh.shape["fs"], 4, 2),
        ("grp", "fs", "tp_0", "tp_1"),
    )
    return jax.shard_map(
        per_device,
        mesh=finer,
        in_specs=(
            P(("grp", "fs"), TP),
            P(None, TP),
            P("fs", TP),
            P("fs", TP),
            P(TP, "fs"),
            P(None, TP),
            P("fs", TP),
            P("fs", TP),
            P(TP, None, None),
            P(None, TP),
            P(TP, "fs"),
            P(None, TP),
        ),
        out_specs=P(("grp", "fs"), TP),
        check_vma=False,
    )
```

profile of v0, /device:TPU:33, one launch (start us, length us, event | category | flops | bytes accessed | tf_op | source)
XLA Modules:
  0.0 387.3 jit_solution(81376959434211735)
XLA Ops:
  6.6 1.8 pad_maximum_fusion
  8.5 0.7 all-gather.6.cloned.1.call-update
  9.2 1.0 pad_maximum_fusion.1
  10.3 13.3 %all_to_all.50 = bf16[4,385,256]{2,1,0:T(8,128)(2,1)S(1)} all-to-all(bf16[4,385,256]{2,1,0:T(8,128)(2,1)S(1)} %broadcast_in_dim.91), channel_id=1, replica_groups=mesh['grp'=2,'fs'=16,'tp_0'=4,'tp_1'=2] {'tp_0'}, dimensions={0} | all-to-all | bytes 1576960 | tf_op jit(solution)/shard_map/all_to_all | solution.py:12
  23.9 0.4 broadcast_in_dim.92
  24.3 23.7 %all_to_all.51 = bf16[2,4,385,256]{3,1,2,0:T(4,128)(2,1)S(1)} all-to-all(bf16[2,4,385,256]{3,1,2,0:T(4,128)(2,1)S(1)} %broadcast_in_dim.92), channel_id=1, replica_groups=mesh['grp'=2,'fs'=16,'tp_0'=4,'tp_1'=2] {'tp_1'}, dimensions={0} | all-to-all | bytes 3153920 | tf_op jit(solution)/shard_map/all_to_all | solution.py:12
  48.2 1.9 slice_convert_fusion.2
  50.2 3.6 copy.35
  54.1 2.3 fusion.2
  56.4 48.7 %all-gather.4.cloned.1.call-done = bf16[2048,1536]{1,0:T(8,128)(2,1)} async-done(((bf16[128,1536]{1,0:T(8,128)(2,1)}), bf16[2048,1536]{1,0:T(8,128)(2,1)}) %all-gather.4.cloned.1.call-update) | async-done | bytes 6291472 | tf_op jit(solution)/shard_map/all_gather | solution.py:54
  105.1 4.3 %fusion.11 = f32[384,768]{1,0:T(8,128)} fusion(bf16[384,2048]{0,1:T(8,128)(2,1)S(1)} %fusion.2, bf16[2048,1536]{1,0:T(8,128)(2,1)} %all-gather.4.cloned.1.call-done, f32[384]{0:T(512)S(1)} %add_rsqrt_fusion.2), kind=kOutput, calls=%fused_computation.29 | convolution fusion | flops 1208254464 | bytes 5899776 | tf_op jit(solution)/shard_map/dot_general | solution.py:99
  109.4 71.1 %all-gather.6.cloned.1.call-done = bf16[768,2048]{1,0:T(8,128)(2,1)} async-done(((bf16[768,128]{1,0:T(8,128)(2,1)}), bf16[768,2048]{1,0:T(8,128)(2,1)}) %all-gather.6.cloned.1.call-update) | async-done | bytes 3145744 | tf_op jit(solution)/shard_map/all_gather | solution.py:95
  180.5 6.4 %convolution_convert_fusion.1 = bf16[384,2048]{1,0:T(8,128)(2,1)S(1)} fusion(bf16[768,2048]{1,0:T(8,128)(2,1)} %all-gather.6.cloned.1.call-done, bf16[384,2048]{0,1:T(8,128)(2,1)S(1)} %fusion.2, bf16[2048,1536]{1,0:T(8,128)(2,1)} %all-gather.4.cloned.1.call-done, f32[384,768]{1,0:T(8,128)} %fusion.11, f32[384]{0:T(512)S(1)} %add_rsqrt_fusion.2), kind=kOutput, calls=%fused_computation.13 | convolution fusion | flops 2418769920 | bytes 10618368 | tf_op jit(solution)/shard_map/dot_general | solution.py:102
  186.9 1.3 copy.58
  188.1 15.3 %all-to-all-start.2 = ((bf16[8,384,256]{2,1,0:T(8,128)(2,1)}), bf16[8,384,256]{2,1,0:T(8,128)(2,1)S(1)}, u32[]{:S(2)}, u32[]{:S(2)}) async-start(bf16[8,384,256]{2,1,0:T(8,128)(2,1)} %bitcast.111), calls=%async_computation.2 | async-start | bytes 3145728 | tf_op jit(solution)/shard_map/all_to_all | solution.py:44
  203.5 0.7 pad_maximum_fusion.4
  204.2 19.8 %all-to-all-done.2 = bf16[8,384,256]{2,1,0:T(8,128)(2,1)S(1)} async-done(((bf16[8,384,256]{2,1,0:T(8,128)(2,1)}), bf16[8,384,256]{2,1,0:T(8,128)(2,1)S(1)}, u32[]{:S(2)}, u32[]{:S(2)}) %all-to-all-start.2) | async-done | bytes 1572896 | tf_op jit(solution)/shard_map/all_to_all | solution.py:44
  224.4 0.9 broadcast_in_dim.93
  225.3 3.6 all-to-all-start.3
  229.1 11.3 %all-to-all-done.3 = bf16[4,385,256]{2,1,0:T(8,128)(2,1)S(1)} async-done(((bf16[4,385,256]{2,1,0:T(8,128)(2,1)}), bf16[4,385,256]{2,1,0:T(8,128)(2,1)S(1)}, u32[]{:S(2)}, u32[]{:S(2)}) %all-to-all-start.3) | async-done | bytes 788512 | tf_op jit(solution)/shard_map/all_to_all | solution.py:12
  240.7 0.4 broadcast_in_dim.94
  241.1 6.5 %all_to_all.52 = bf16[2,4,385,256]{3,1,2,0:T(4,128)(2,1)S(1)} all-to-all(bf16[2,4,385,256]{3,1,2,0:T(4,128)(2,1)S(1)} %broadcast_in_dim.94), channel_id=1, replica_groups=mesh['grp'=2,'fs'=16,'tp_0'=4,'tp_1'=2] {'tp_1'}, dimensions={0} | all-to-all | bytes 3153920 | tf_op jit(solution)/shard_map/all_to_all | solution.py:12
  247.6 0.9 broadcast_in_dim.104
  248.5 7.0 %all-to-all-start.5 = ((bf16[16,128,128]{1,2,0:T(8,128)(2,1)}), bf16[16,128,128]{1,2,0:T(8,128)(2,1)}, u32[]{:S(2)}, u32[]{:S(2)}) async-start(bf16[16,128,128]{1,2,0:T(8,128)(2,1)} %broadcast_in_dim.104), calls=%async_computation.5 | async-start | bytes 1048576 | tf_op jit(solution)/shard_map/all_to_all | solution.py:12
  255.7 1.9 slice_convert_fusion.1
  257.6 3.5 copy.39
  261.5 2.2 fusion.1
  263.8 3.6 all-gather.8.cloned.1.call-done
  267.4 1.6 fusion.47
  269.1 0.7 copy-done.6
  270.0 0.7 fusion.73
  270.7 10.8 %all-to-all-done.5 = bf16[16,128,128]{1,2,0:T(8,128)(2,1)} async-done(((bf16[16,128,128]{1,2,0:T(8,128)(2,1)}), bf16[16,128,128]{1,2,0:T(8,128)(2,1)}, u32[]{:S(2)}, u32[]{:S(2)}) %all-to-all-start.5) | async-done | bytes 524320 | tf_op jit(solution)/shard_map/all_to_all | solution.py:12
  281.5 2.4 convolution_convert_fusion.2
  284.0 31.3 %all_to_all.53 = bf16[8,384,256]{2,1,0:T(8,128)(2,1)S(1)} all-to-all(bf16[8,384,256]{2,1,0:T(8,128)(2,1)S(1)} %bitcast.125), channel_id=1, replica_groups=mesh['grp'=2,'fs'=16,'tp_0'=4,'tp_1'=2] {'tp_0','tp_1'}, dimensions={0} | all-to-all | bytes 3145728 | tf_op jit(solution)/shard_map/all_to_all | solution.py:44
  315.5 1.2 copy-done.12
  316.7 0.7 fusion.41
  317.4 0.6 copy-done.4
  318.1 13.9 %all_to_all.54 = bf16[4,385,256]{2,1,0:T(8,128)(2,1)S(1)} all-to-all(bf16[4,385,256]{2,1,0:T(8,128)(2,1)S(1)} %broadcast_in_dim.105), channel_id=1, replica_groups=mesh['grp'=2,'fs'=16,'tp_0'=4,'tp_1'=2] {'tp_0'}, dimensions={0} | all-to-all | bytes 1576960 | tf_op jit(solution)/shard_map/all_to_all | solution.py:12
  332.3 0.4 broadcast_in_dim.106
  332.7 6.5 %all_to_all.55 = bf16[2,4,385,256]{3,1,2,0:T(4,128)(2,1)S(1)} all-to-all(bf16[2,4,385,256]{3,1,2,0:T(4,128)(2,1)S(1)} %broadcast_in_dim.106), channel_id=1, replica_groups=mesh['grp'=2,'fs'=16,'tp_0'=4,'tp_1'=2] {'tp_1'}, dimensions={0} | all-to-all | bytes 3153920 | tf_op jit(solution)/shard_map/all_to_all | solution.py:12
  339.5 1.9 slice_convert_fusion
  341.8 2.4 copy.46
  344.6 1.2 copy-done.2
  345.7 3.3 fusion.14
  349.1 6.5 %convolution_convert_fusion = bf16[384,2048]{1,0:T(8,128)(2,1)S(1)} fusion(bf16[768,2048]{1,0:T(8,128)(2,1)} %all-gather.6.cloned.1.call-done, bf16[384,2048]{0,1:T(8,128)(2,1)} %copy-done.2, bf16[2048,1536]{1,0:T(8,128)(2,1)} %all-gather.4.cloned.1.call-done, f32[384,768]{1,0:T(8,128)S(1)} %fusion.14, f32[384]{0:T(512)S(1)} %add_rsqrt_fusion), kind=kOutput, calls=%fused_computation.12 | convolution fusion | flops 2418769920 | bytes 10618368 | tf_op jit(solution)/shard_map/dot_general | solution.py:102
  355.7 23.4 %all_to_all.56 = bf16[8,384,256]{2,1,0:T(8,128)(2,1)S(1)} all-to-all(bf16[8,384,256]{2,1,0:T(8,128)(2,1)S(1)} %bitcast.126), channel_id=1, replica_groups=mesh['grp'=2,'fs'=16,'tp_0'=4,'tp_1'=2] {'tp_0','tp_1'}, dimensions={0} | all-to-all | bytes 3145728 | tf_op jit(solution)/shard_map/all_to_all | solution.py:44
  379.3 0.7 copy-done.5
  380.0 0.7 add_convert_fusion
  (63 shorter events, 4.8 us)
Async XLA Ops:
  6.5 275.0 %copy-start = (bf16[1,128,128]{2,1,0:T(8,128)(2,1)S(1)}, bf16[1,128,128]{2,1,0:T(8,128)(2,1)}, u32[]{:S(2)}) copy-start(bf16[1,128,128]{2,1,0:T(8,128)(2,1)} %param.20) | copy-start | bytes 98308
  6.6 98.6 %all-gather.4.cloned.1.call-start = ((), (), s32[]{:S(2)}) async-start(), calls=%async_computation.10 | async-start | bytes 6684672 | tf_op jit(solution)/shard_map/all_gather | solution.py:54
  8.4 172.1 %all-gather.6.cloned.1.call-start = ((), (), s32[]{:S(2)}) async-start(), calls=%async_computation.11 | async-start | bytes 3342336 | tf_op jit(solution)/shard_map/all_gather | solution.py:95
  188.1 15.4 %copy-start.7 = (bf16[128,256]{1,0:T(8,128)(2,1)S(1)}, bf16[128,256]{1,0:T(8,128)(2,1)}, u32[]{:S(2)}) copy-start(bf16[128,256]{1,0:T(8,128)(2,1)} %param.19) | copy-start | bytes 196612
  188.1 15.4 %copy-start.9 = (bf16[128,128]{1,0:T(8,128)(2,1)S(1)}, bf16[128,128]{1,0:T(8,128)(2,1)}, u32[]{:S(2)}) copy-start(bf16[128,128]{1,0:T(8,128)(2,1)} %param.18) | copy-start | bytes 98308
  188.1 35.9 %all-to-all-start.2 = ((bf16[8,384,256]{2,1,0:T(8,128)(2,1)}), bf16[8,384,256]{2,1,0:T(8,128)(2,1)S(1)}, u32[]{:S(2)}, u32[]{:S(2)}) async-start(bf16[8,384,256]{2,1,0:T(8,128)(2,1)} %bitcast.111), calls=%async_computation.2 | async-start | bytes 3145728 | tf_op jit(solution)/shard_map/all_to_all | solution.py:44
  203.4 20.8 %copy-start.3 = (bf16[384,256]{1,0:T(8,128)(2,1)S(1)}, bf16[384,256]{1,0:T(8,128)(2,1)}, u32[]{:S(2)}) copy-start(bf16[384,256]{1,0:T(8,128)(2,1)} %param.12) | copy-start | bytes 589828
  203.4 20.9 %copy-start.10 = (bf16[1,256]{1,0:T(2,128)(2,1)S(1)}, bf16[1,256]{1,0:T(2,128)(2,1)}, u32[]{:S(2)}) copy-start(bf16[1,256]{1,0:T(2,128)(2,1)} %param.17) | copy-start | bytes 1540
  203.4 64.0 %all-gather.8.cloned.1.call-start = ((), (), s32[]{:S(2)}) async-start(), calls=%async_computation.12 | async-start | bytes 1671168 | tf_op jit(solution)/shard_map/all_gather | solution.py:54
  224.3 4.6 %copy-start.8 = (bf16[128,128]{1,0:T(8,128)(2,1)S(1)}, bf16[128,128]{1,0:T(8,128)(2,1)}, u32[]{:S(2)}) copy-start(bf16[128,128]{1,0:T(8,128)(2,1)} %param.22) | copy-start | bytes 98308
  225.3 15.1 %all-to-all-start.3 = ((bf16[4,385,256]{2,1,0:T(8,128)(2,1)}), bf16[4,385,256]{2,1,0:T(8,128)(2,1)S(1)}, u32[]{:S(2)}, u32[]{:S(2)}) async-start(bf16[4,385,256]{2,1,0:T(8,128)(2,1)} %broadcast_in_dim.93), calls=%async_computation.3 | async-start | bytes 1605632 | tf_op jit(solution)/shard_map/all_to_all | solution.py:12
  248.5 33.0 %all-to-all-start.5 = ((bf16[16,128,128]{1,2,0:T(8,128)(2,1)}), bf16[16,128,128]{1,2,0:T(8,128)(2,1)}, u32[]{:S(2)}, u32[]{:S(2)}) async-start(bf16[16,128,128]{1,2,0:T(8,128)(2,1)} %broadcast_in_dim.104), calls=%async_computation.5 | async-start | bytes 1048576 | tf_op jit(solution)/shard_map/all_to_all | solution.py:12
  269.1 0.7 copy-start.6
  269.1 12.4 %copy-start.13 = (f32[1,128]{1,0:T(1,128)S(1)}, f32[1,128]{1,0:T(1,128)}, u32[]{:S(2)}) copy-start(f32[1,128]{1,0:T(1,128)} %param.21) | copy-start | bytes 1540
  315.3 1.4 copy-start.12
  316.7 0.7 copy-start.11
  317.4 0.7 copy-start.4
  344.6 1.2 copy-start.2
  355.7 25.1 %copy-start.1 = (bf16[1,128,128]{2,1,0:T(8,128)(2,1)S(1)}, bf16[1,128,128]{2,1,0:T(8,128)(2,1)}, u32[]{:S(2)}) copy-start(bf16[1,128,128]{2,1,0:T(8,128)(2,1)} %param.20) | copy-start | bytes 98308
  379.1 0.9 copy-start.5
Sparse Core Ops, SparseCore 0:
  9.1 95.9 all-gather.3
  106.8 73.5 all-gather.5
  206.1 61.3 all-gather.7
where the time goes:
time: 388 us; the launch traced here: 387 us
  waiting for transfers between devices  166 us (43%)
  blocking collectives  119 us (31%)
  starting transfers between devices  26 us (7%)
  matrix products  25.2 us (6%)
  local copies, waits for them, and re-layouts  20.2 us (5%)
  other arithmetic  17.6 us (5%)
  between operations  13.6 us (4%)
    all_gather x1, waiting for transfers between devices, per_device(): down_whole = lax.all_gather(ffn_down_w, 'fs', axis=1, tiled=True)  71.1 us
    all_to_all x5, blocking collectives, from_everyone(): lax.all_to_all(jnp.broadcast_to(value[None], (length, *value.shape)), axi...  64 us
    all_to_all x2, blocking collectives, summed_on_arrival(): lax.all_to_all(tiles, axis, split_axis=0, concat_axis=0, tiled=True)  54.7 us
    all_gather x2, waiting for transfers between devices, sent_together(): lax.all_gather(both, axis, axis=dim, tiled=True)  52.3 us
    all_to_all x2, waiting for transfers between devices, from_everyone(): lax.all_to_all(jnp.broadcast_to(value[None], (length, *value.shape)), axi...  22.1 us
    all_to_all x1, waiting for transfers between devices, summed_on_arrival(): lax.all_to_all(tiles, axis, split_axis=0, concat_axis=0, tiled=True)  19.8 us
    all_to_all x1, starting transfers between devices, summed_on_arrival(): lax.all_to_all(tiles, axis, split_axis=0, concat_axis=0, tiled=True)  15.3 us
    dot_general x2, matrix products, feed_forward(): return jnp.dot(hidden, down_whole, preferred_element_type=jnp.float32)  12.9 us
  transfers between devices with their start and end apart: 6, of which 6 were waited for; matrix products, arithmetic and copies ran while one was open for 7% of the time, Pallas kernels for 0%

commit v1 on v0

--- a/solution.py
+++ b/solution.py
@@ -92,7 +92,14 @@
 ):
     row_count = layer_input.shape[0]
     gate_whole, up_whole = sent_together((ffn_gate_w, ffn_up_w), "fs", 0, 1)
-    down_whole = lax.all_gather(ffn_down_w, "fs", axis=1, tiled=True)
+
+    def recast_view_all(u_in):
+        val = lax.axis_size("fs")
+        block_next = jnp.stack(val * [u_in], 0)
+        row_out = lax.all_to_all(block_next, "fs", 0, 0)
+        return jnp.concatenate(row_out, axis=1)
+
+    down_whole = recast_view_all(ffn_down_w)
 
     def feed_forward(values, gain):
         scaled, factor = norm_rows(values, gain)

time: 388 us -> 452 us (1.16)
  waiting for transfers between devices: 166 us -> 234 us
  blocking collectives: 119 us -> 105 us
  starting transfers between devices: 26 us -> 33.2 us
    all_gather x2, waiting for transfers between devices: 52.3 us -> 184 us  [sent_together(): lax.all_gather(both, axis, axis=dim, tiled=True)]
    all_gather x1 -> x0, waiting for transfers between devices: 71.1 us -> none  [per_device(): down_whole = lax.all_gather(ffn_down_w, 'fs', axis=1, tiled=True)]
    all_to_all x5 -> x4, blocking collectives: 64 us -> 51.5 us  [from_everyone(): lax.all_to_all(jnp.broadcast_to(value[None], (length, *value.shape)), axi...]
    all_to_all x0 -> x1, starting transfers between devices: none -> 8.75 us  [recast_view_all(): row_out = lax.all_to_all(block_next, 'fs', 0, 0)]
    all_to_all x1, starting transfers between devices: 15.3 us -> 7.76 us  [summed_on_arrival(): lax.all_to_all(tiles, axis, split_axis=0, concat_axis=0, tiled=True)]
    all_to_all x2 -> x3, waiting for transfers between devices: 22.1 us -> 29.6 us  [from_everyone(): lax.all_to_all(jnp.broadcast_to(value[None], (length, *value.shape)), axi...]
    all_to_all x2 -> x3, starting transfers between devices: 10.5 us -> 16.7 us  [from_everyone(): lax.all_to_all(jnp.broadcast_to(value[None], (length, *value.shape)), axi...]
  transfers between devices with their start and end apart: 6 -> 7, of which waited for: 6 -> 6; matrix products, arithmetic and copies ran while one was open for 7% -> 7% of each run, Pallas kernels for 0% -> 0%
where the time goes in v1:
time: 452 us; the launch traced here: 451 us
  waiting for transfers between devices  234 us (52%)
  blocking collectives  105 us (23%)
  starting transfers between devices  33.2 us (7%)
  matrix products  25.3 us (6%)
  local copies, waits for them, and re-layouts  23.2 us (5%)
  other arithmetic  16.6 us (4%)
  between operations  13.9 us (3%)
    all_gather x2, waiting for transfers between devices, sent_together(): lax.all_gather(both, axis, axis=dim, tiled=True)  184 us
    all_to_all x2, blocking collectives, summed_on_arrival(): lax.all_to_all(tiles, axis, split_axis=0, concat_axis=0, tiled=True)  53.9 us
    all_to_all x4, blocking collectives, from_everyone(): lax.all_to_all(jnp.broadcast_to(value[None], (length, *value.shape)), axi...  51.5 us
    all_to_all x3, waiting for transfers between devices, from_everyone(): lax.all_to_all(jnp.broadcast_to(value[None], (length, *value.shape)), axi...  29.6 us
    all_to_all x1, waiting for transfers between devices, summed_on_arrival(): lax.all_to_all(tiles, axis, split_axis=0, concat_axis=0, tiled=True)  19.8 us
    all_to_all x3, starting transfers between devices, from_everyone(): lax.all_to_all(jnp.broadcast_to(value[None], (length, *value.shape)), axi...  16.7 us
    dot_general x2, matrix products, feed_forward(): return jnp.dot(hidden, down_whole, preferred_element_type=jnp.float32)  12.9 us
    convert_element_type x3, local copies, waits for them, and re-layouts, norm_rows(): widened = gathered.astype(jnp.float32)  9.45 us
  transfers between devices with their start and end apart: 7, of which 6 were waited for; matrix products, arithmetic and copies ran while one was open for 7% of the time, Pallas kernels for 0%

profile of v1, /device:TPU:33, one launch (start us, length us, event | category | flops | bytes accessed | tf_op | source)
XLA Modules:
  0.0 451.2 jit_solution(1848715493392555394)
XLA Ops:
  6.6 1.0 pad_maximum_fusion.1
  7.6 1.0 broadcast_in_dim.91
  8.5 5.2 %all-to-all-start = ((bf16[4,385,256]{2,1,0:T(8,128)(2,1)}), bf16[4,385,256]{2,1,0:T(8,128)(2,1)S(1)}, u32[]{:S(2)}, u32[]{:S(2)}) async-start(bf16[4,385,256]{2,1,0:T(8,128)(2,1)} %broadcast_in_dim.91), calls=%async_computation | async-start | bytes 1605632 | tf_op jit(solution)/shard_map/all_to_all | solution.py:12
  13.8 0.8 pad_maximum_fusion
  14.8 7.4 %all-to-all-done = bf16[4,385,256]{2,1,0:T(8,128)(2,1)S(1)} async-done(((bf16[4,385,256]{2,1,0:T(8,128)(2,1)}), bf16[4,385,256]{2,1,0:T(8,128)(2,1)S(1)}, u32[]{:S(2)}, u32[]{:S(2)}) %all-to-all-start) | async-done | bytes 788512 | tf_op jit(solution)/shard_map/all_to_all | solution.py:12
  22.9 24.6 %all_to_all.55 = bf16[2,4,385,256]{3,1,2,0:T(4,128)(2,1)S(1)} all-to-all(bf16[2,4,385,256]{3,1,2,0:T(4,128)(2,1)S(1)} %broadcast_in_dim.92), channel_id=1, replica_groups=mesh['grp'=2,'fs'=16,'tp_0'=4,'tp_1'=2] {'tp_1'}, dimensions={0} | all-to-all | bytes 3153920 | tf_op jit(solution)/shard_map/all_to_all | solution.py:12
  47.5 2.0 stack.2
  49.5 8.8 %all-to-all-start.2 = ((bf16[16,768,128]{1,2,0:T(8,128)(2,1)}), bf16[16,768,128]{1,2,0:T(8,128)(2,1)}, u32[]{:S(2)}, u32[]{:S(2)}) async-start(bf16[16,768,128]{1,2,0:T(8,128)(2,1)} %stack.2), calls=%async_computation.2 | async-start | bytes 6291456 | tf_op jit(solution)/shard_map/all_to_all | solution.py:99
  58.4 1.9 slice_convert_fusion.2
  60.4 3.6 copy.37
  64.3 2.2 fusion.2
  66.6 180.5 %all-gather.3.cloned.1.call-done = bf16[2048,1536]{1,0:T(8,128)(2,1)} async-done(((bf16[128,1536]{1,0:T(8,128)(2,1)}), bf16[2048,1536]{1,0:T(8,128)(2,1)}) %all-gather.3.cloned.1.call-update) | async-done | bytes 6291472 | tf_op jit(solution)/shard_map/all_gather | solution.py:54
  247.1 4.4 fusion.11
  251.5 6.4 %convolution_convert_fusion.1 = bf16[384,2048]{1,0:T(8,128)(2,1)S(1)} fusion(bf16[768,2048]{0,1:T(8,128)(2,1)} %bitcast.7, bf16[384,2048]{0,1:T(8,128)(2,1)S(1)} %fusion.2, bf16[2048,1536]{1,0:T(8,128)(2,1)} %all-gather.3.cloned.1.call-done, f32[384,768]{1,0:T(8,128)} %fusion.11, f32[384]{0:T(512)S(1)} %add_rsqrt_fusion.2), kind=kOutput, calls=%fused_computation.13 | convolution fusion | flops 2418769920 | bytes 10618368 | tf_op jit(solution)/shard_map/dot_general | solution.py:109
  257.9 1.3 copy.61
  259.1 7.8 %all-to-all-start.3 = ((bf16[8,384,256]{2,1,0:T(8,128)(2,1)}), bf16[8,384,256]{2,1,0:T(8,128)(2,1)S(1)}, u32[]{:S(2)}, u32[]{:S(2)}) async-start(bf16[8,384,256]{2,1,0:T(8,128)(2,1)} %bitcast.114), calls=%async_computation.3 | async-start | bytes 3145728 | tf_op jit(solution)/shard_map/all_to_all | solution.py:44
  267.0 0.7 pad_maximum_fusion.4
  267.7 19.8 %all-to-all-done.3 = bf16[8,384,256]{2,1,0:T(8,128)(2,1)S(1)} async-done(((bf16[8,384,256]{2,1,0:T(8,128)(2,1)}), bf16[8,384,256]{2,1,0:T(8,128)(2,1)S(1)}, u32[]{:S(2)}, u32[]{:S(2)}) %all-to-all-start.3) | async-done | bytes 1572896 | tf_op jit(solution)/shard_map/all_to_all | solution.py:44
  287.8 0.9 broadcast_in_dim.93
  288.7 3.6 all-to-all-start.4
  292.5 11.3 %all-to-all-done.4 = bf16[4,385,256]{2,1,0:T(8,128)(2,1)S(1)} async-done(((bf16[4,385,256]{2,1,0:T(8,128)(2,1)}), bf16[4,385,256]{2,1,0:T(8,128)(2,1)S(1)}, u32[]{:S(2)}, u32[]{:S(2)}) %all-to-all-start.4) | async-done | bytes 788512 | tf_op jit(solution)/shard_map/all_to_all | solution.py:12
  304.1 0.4 broadcast_in_dim.94
  304.6 6.5 %all_to_all.56 = bf16[2,4,385,256]{3,1,2,0:T(4,128)(2,1)S(1)} all-to-all(bf16[2,4,385,256]{3,1,2,0:T(4,128)(2,1)S(1)} %broadcast_in_dim.94), channel_id=1, replica_groups=mesh['grp'=2,'fs'=16,'tp_0'=4,'tp_1'=2] {'tp_1'}, dimensions={0} | all-to-all | bytes 3153920 | tf_op jit(solution)/shard_map/all_to_all | solution.py:12
  311.0 0.9 broadcast_in_dim.104
  312.0 7.8 %all-to-all-start.6 = ((bf16[16,128,128]{1,2,0:T(8,128)(2,1)}), bf16[16,128,128]{1,2,0:T(8,128)(2,1)}, u32[]{:S(2)}, u32[]{:S(2)}) async-start(bf16[16,128,128]{1,2,0:T(8,128)(2,1)} %broadcast_in_dim.104), calls=%async_computation.6 | async-start | bytes 1048576 | tf_op jit(solution)/shard_map/all_to_all | solution.py:12
  320.0 1.9 slice_convert_fusion.1
  321.9 3.5 copy.42
  325.9 2.2 fusion.1
  328.1 3.6 all-gather.5.cloned.1.call-done
  331.7 1.6 fusion.47
  333.4 0.7 copy-done.6
  334.3 0.7 fusion.73
  335.0 10.9 %all-to-all-done.6 = bf16[16,128,128]{1,2,0:T(8,128)(2,1)} async-done(((bf16[16,128,128]{1,2,0:T(8,128)(2,1)}), bf16[16,128,128]{1,2,0:T(8,128)(2,1)}, u32[]{:S(2)}, u32[]{:S(2)}) %all-to-all-start.6) | async-done | bytes 524320 | tf_op jit(solution)/shard_map/all_to_all | solution.py:12
  345.8 2.4 convolution_convert_fusion.2
  348.3 30.5 %all_to_all.57 = bf16[8,384,256]{2,1,0:T(8,128)(2,1)S(1)} all-to-all(bf16[8,384,256]{2,1,0:T(8,128)(2,1)S(1)} %bitcast.128), channel_id=1, replica_groups=mesh['grp'=2,'fs'=16,'tp_0'=4,'tp_1'=2] {'tp_0','tp_1'}, dimensions={0} | all-to-all | bytes 3145728 | tf_op jit(solution)/shard_map/all_to_all | solution.py:44
  379.0 1.2 copy-done.15
  380.2 0.7 fusion.41
  381.0 0.6 copy-done.4
  381.7 13.9 %all_to_all.58 = bf16[4,385,256]{2,1,0:T(8,128)(2,1)S(1)} all-to-all(bf16[4,385,256]{2,1,0:T(8,128)(2,1)S(1)} %broadcast_in_dim.105), channel_id=1, replica_groups=mesh['grp'=2,'fs'=16,'tp_0'=4,'tp_1'=2] {'tp_0'}, dimensions={0} | all-to-all | bytes 1576960 | tf_op jit(solution)/shard_map/all_to_all | solution.py:12
  396.3 6.5 %all_to_all.59 = bf16[2,4,385,256]{3,1,2,0:T(4,128)(2,1)S(1)} all-to-all(bf16[2,4,385,256]{3,1,2,0:T(4,128)(2,1)S(1)} %broadcast_in_dim.106), channel_id=1, replica_groups=mesh['grp'=2,'fs'=16,'tp_0'=4,'tp_1'=2] {'tp_1'}, dimensions={0} | all-to-all | bytes 3153920 | tf_op jit(solution)/shard_map/all_to_all | solution.py:12
  403.1 1.9 slice_convert_fusion
  405.4 2.4 copy.49
  408.1 1.1 copy-done.2
  409.3 3.3 fusion.14
  412.6 6.5 %convolution_convert_fusion = bf16[384,2048]{1,0:T(8,128)(2,1)S(1)} fusion(bf16[768,2048]{0,1:T(8,128)(2,1)} %bitcast.7, bf16[384,2048]{0,1:T(8,128)(2,1)} %copy-done.2, bf16[2048,1536]{1,0:T(8,128)(2,1)} %all-gather.3.cloned.1.call-done, f32[384,768]{1,0:T(8,128)S(1)} %fusion.14, f32[384]{0:T(512)S(1)} %add_rsqrt_fusion), kind=kOutput, calls=%fused_computation.12 | convolution fusion | flops 2418769920 | bytes 10618368 | tf_op jit(solution)/shard_map/dot_general | solution.py:109
  419.2 23.4 %all_to_all.60 = bf16[8,384,256]{2,1,0:T(8,128)(2,1)S(1)} all-to-all(bf16[8,384,256]{2,1,0:T(8,128)(2,1)S(1)} %bitcast.129), channel_id=1, replica_groups=mesh['grp'=2,'fs'=16,'tp_0'=4,'tp_1'=2] {'tp_0','tp_1'}, dimensions={0} | all-to-all | bytes 3145728 | tf_op jit(solution)/shard_map/all_to_all | solution.py:44
  442.9 0.7 copy-done.5
  443.6 0.7 add_convert_fusion
  (71 shorter events, 5.6 us)
Async XLA Ops:
  6.5 339.3 %copy-start = (bf16[1,128,128]{2,1,0:T(8,128)(2,1)S(1)}, bf16[1,128,128]{2,1,0:T(8,128)(2,1)}, u32[]{:S(2)}) copy-start(bf16[1,128,128]{2,1,0:T(8,128)(2,1)} %param.20) | copy-start | bytes 98308
  6.6 7.2 %copy-start.9 = (bf16[128,768]{1,0:T(8,128)(2,1)S(1)}, bf16[128,768]{1,0:T(8,128)(2,1)}, u32[]{:S(2)}) copy-start(bf16[128,768]{1,0:T(8,128)(2,1)} %param.14) | copy-start | bytes 589828
  6.6 7.2 %copy-start.8 = (bf16[128,768]{1,0:T(8,128)(2,1)S(1)}, bf16[128,768]{1,0:T(8,128)(2,1)}, u32[]{:S(2)}) copy-start(bf16[128,768]{1,0:T(8,128)(2,1)} %param.15) | copy-start | bytes 589828
  8.5 6.1 %copy-start.7 = (bf16[768,128]{1,0:T(8,128)(2,1)S(1)}, bf16[768,128]{1,0:T(8,128)(2,1)}, u32[]{:S(2)}) copy-start(bf16[768,128]{1,0:T(8,128)(2,1)} %param.16) | copy-start | bytes 589828
  8.5 13.7 %all-to-all-start = ((bf16[4,385,256]{2,1,0:T(8,128)(2,1)}), bf16[4,385,256]{2,1,0:T(8,128)(2,1)S(1)}, u32[]{:S(2)}, u32[]{:S(2)}) async-start(bf16[4,385,256]{2,1,0:T(8,128)(2,1)} %broadcast_in_dim.91), calls=%async_computation | async-start | bytes 1605632 | tf_op jit(solution)/shard_map/all_to_all | solution.py:12
  13.8 233.3 %all-gather.3.cloned.1.call-start = ((), (), s32[]{:S(2)}) async-start(), calls=%async_computation.11 | async-start | bytes 6684672 | tf_op jit(solution)/shard_map/all_gather | solution.py:54
  49.5 202.0 %all-to-all-start.2 = ((bf16[16,768,128]{1,2,0:T(8,128)(2,1)}), bf16[16,768,128]{1,2,0:T(8,128)(2,1)}, u32[]{:S(2)}, u32[]{:S(2)}) async-start(bf16[16,768,128]{1,2,0:T(8,128)(2,1)} %stack.2), calls=%async_computation.2 | async-start | bytes 6291456 | tf_op jit(solution)/shard_map/all_to_all | solution.py:99
  259.1 7.8 %copy-start.10 = (bf16[128,256]{1,0:T(8,128)(2,1)S(1)}, bf16[128,256]{1,0:T(8,128)(2,1)}, u32[]{:S(2)}) copy-start(bf16[128,256]{1,0:T(8,128)(2,1)} %param.19) | copy-start | bytes 196612
  259.1 7.8 %copy-start.12 = (bf16[128,128]{1,0:T(8,128)(2,1)S(1)}, bf16[128,128]{1,0:T(8,128)(2,1)}, u32[]{:S(2)}) copy-start(bf16[128,128]{1,0:T(8,128)(2,1)} %param.18) | copy-start | bytes 98308
  259.1 28.3 %all-to-all-start.3 = ((bf16[8,384,256]{2,1,0:T(8,128)(2,1)}), bf16[8,384,256]{2,1,0:T(8,128)(2,1)S(1)}, u32[]{:S(2)}, u32[]{:S(2)}) async-start(bf16[8,384,256]{2,1,0:T(8,128)(2,1)} %bitcast.114), calls=%async_computation.3 | async-start | bytes 3145728 | tf_op jit(solution)/shard_map/all_to_all | solution.py:44
  266.9 20.8 %copy-start.3 = (bf16[384,256]{1,0:T(8,128)(2,1)S(1)}, bf16[384,256]{1,0:T(8,128)(2,1)}, u32[]{:S(2)}) copy-start(bf16[384,256]{1,0:T(8,128)(2,1)} %param.12) | copy-start | bytes 589828
  266.9 20.9 %copy-start.13 = (bf16[1,256]{1,0:T(2,128)(2,1)S(1)}, bf16[1,256]{1,0:T(2,128)(2,1)}, u32[]{:S(2)}) copy-start(bf16[1,256]{1,0:T(2,128)(2,1)} %param.17) | copy-start | bytes 1540
  266.9 64.8 %all-gather.5.cloned.1.call-start = ((), (), s32[]{:S(2)}) async-start(), calls=%async_computation.12 | async-start | bytes 1671168 | tf_op jit(solution)/shard_map/all_gather | solution.py:54
  287.8 4.6 %copy-start.11 = (bf16[128,128]{1,0:T(8,128)(2,1)S(1)}, bf16[128,128]{1,0:T(8,128)(2,1)}, u32[]{:S(2)}) copy-start(bf16[128,128]{1,0:T(8,128)(2,1)} %param.22) | copy-start | bytes 98308
  288.7 15.1 %all-to-all-start.4 = ((bf16[4,385,256]{2,1,0:T(8,128)(2,1)}), bf16[4,385,256]{2,1,0:T(8,128)(2,1)S(1)}, u32[]{:S(2)}, u32[]{:S(2)}) async-start(bf16[4,385,256]{2,1,0:T(8,128)(2,1)} %broadcast_in_dim.93), calls=%async_computation.4 | async-start | bytes 1605632 | tf_op jit(solution)/shard_map/all_to_all | solution.py:12
  312.0 33.9 %all-to-all-start.6 = ((bf16[16,128,128]{1,2,0:T(8,128)(2,1)}), bf16[16,128,128]{1,2,0:T(8,128)(2,1)}, u32[]{:S(2)}, u32[]{:S(2)}) async-start(bf16[16,128,128]{1,2,0:T(8,128)(2,1)} %broadcast_in_dim.104), calls=%async_computation.6 | async-start | bytes 1048576 | tf_op jit(solution)/shard_map/all_to_all | solution.py:12
  333.4 0.7 copy-start.6
  333.4 12.4 %copy-start.16 = (f32[1,128]{1,0:T(1,128)S(1)}, f32[1,128]{1,0:T(1,128)}, u32[]{:S(2)}) copy-start(f32[1,128]{1,0:T(1,128)} %param.21) | copy-start | bytes 1540
  378.8 1.4 copy-start.15
  380.2 0.7 copy-start.14
  380.9 0.7 copy-start.4
  408.1 1.1 copy-start.2
  419.2 25.1 %copy-start.1 = (bf16[1,128,128]{2,1,0:T(8,128)(2,1)S(1)}, bf16[1,128,128]{2,1,0:T(8,128)(2,1)}, u32[]{:S(2)}) copy-start(bf16[1,128,128]{2,1,0:T(8,128)(2,1)} %param.20) | copy-start | bytes 98308
  442.7 0.9 copy-start.5
Sparse Core Ops, SparseCore 0:
  16.4 230.6 all-gather.2
  269.5 62.1 all-gather.4
